TPU v7x, 256 devices: a 8x8x2 block of a 8x8x16 slice. The times are simulated.
256 devices in a mesh: grp: 2 (over z), ep: 16 (over y, core), tp: 8 (over x).
Axes of the slice: x: 8, y: 8, z: 2, core: 2. Of those that a mesh axis runs over, the one named last changes fastest.
The devices are a block of a 8x8x16 slice.
Arguments:
- tokens: bfloat16 [32768, 1024], P(('grp', 'ep', 'tp')), parts along dimension 0, may hold values from -6 to 6
- norm_gain: float32 [1024], replicated, may hold values from 0.1 to 1.9
- gate_weight: bfloat16 [16, 1024, 3584], P('ep', None, 'tp'), may hold values from -0.1875 to 0.1875
- up_weight: bfloat16 [16, 1024, 3584], P('ep', None, 'tp'), may hold values from -0.1875 to 0.1875
- down_weight: bfloat16 [16, 3584, 1024], P('ep', 'tp'), may hold values from -0.09375 to 0.09375
- expert_ids: int32 [32768, 2], P(('grp', 'ep')), parts along dimension 0, may hold values from 0 to 15, all different within a row; in each aligned block of 128 rows (0 to 127, 128 to 255, ...) at most 20 rows name the same one
- route_weight: float32 [32768, 2], P(('grp', 'ep')), parts along dimension 0, may hold values from 0.2 to 1
Outputs:
- mixed: bfloat16 [32768, 1024], P(('grp', 'ep', 'tp')), parts along dimension 0
There are 2 independent parts, one for each index of `grp`. A program takes and returns all parts, laid end to end along the dimension named above; an argument that names none is the same for every part. Nothing has to cross between parts.
Inputs may be any that keep to these rules, and one draw needn't show every extreme that they name: `expert_ids`: A token's 2 experts differ. In the rows of one device (128 tokens, aligned blocks) no expert is named more than 20 times, and in every draw some expert is named exactly 20 times in some device's rows.
All inputs are finite; a program needn't handle non-finite values.
Results may differ from a plain program's by a relative error of at most 0.015.
Values may be sent and summed in bfloat16 or wider, within the bound.
No kernel may reach another device: no remote copies, remote signals or barrier semaphores. Data moves between devices by JAX's collectives and lax.ppermute only.
A program may use at most 64 MiB of HBM per device.

v0:
```python
import functools

import jax
import jax.numpy as jnp
from jax import lax
from jax.experimental import pallas as pl
from jax.experimental.pallas import tpu as pltpu
from jax.sharding import PartitionSpec as P


TOP_K = 2
CORES = 2
HOP = 2
F32 = jnp.float32
BF16 = jnp.bfloat16
VMEM = pl.BlockSpec(memory_space=pltpu.VMEM)
PARAMS = pltpu.CompilerParams(vmem_limit_bytes=24 * 1024 * 1024)


def norm_kernel(tok, gain, out):
    values = tok[...].astype(F32)
    scaled = values * lax.rsqrt(jnp.mean(values * values, axis=-1, keepdims=True) + 1e-06)
    out[...] = (scaled * gain[...]).astype(BF16)


def dispatch_kernel(place, norm_a, tok_b, gain, meta_a, meta_b, *refs, chips, slots):
    blocks, mix_hi, mix_lo, values = refs[:chips], refs[chips], refs[chips + 1], refs[chips + 2]
    chip, core = place[0], place[1]
    rows = norm_a.shape[0]
    both = CORES * rows
    total = chips * slots
    values[:rows] = norm_a[...]
    norm_kernel(tok_b, gain, values.at[rows:])
    meta = jnp.concatenate([meta_a[...].T, meta_b[...].T], axis=0)
    experts = meta[:, 0:TOP_K].astype(jnp.int32)
    distance = jnp.where(experts % CORES == core, (experts // CORES - chip + chips) % chips, -1)
    lane = lax.broadcasted_iota(jnp.int32, (both, 128), 1)
    hot = [lane == distance[:, k : k + 1] for k in range(TOP_K)]
    named = (hot[0] | hot[1]).astype(F32).astype(BF16)
    earlier = lax.broadcasted_iota(jnp.int32, (both, both), 1) < lax.broadcasted_iota(
        jnp.int32, (both, both), 0
    )
    rank = jnp.dot(earlier.astype(F32).astype(BF16), named, preferred_element_type=F32)
    row = lax.broadcasted_iota(jnp.int32, (both, total), 1)
    here = []
    for k in range(TOP_K):
        slot = jnp.sum(jnp.where(hot[k], rank, 0.0), axis=1, keepdims=True).astype(jnp.int32)
        at = jnp.where(distance[:, k : k + 1] < 0, -1, distance[:, k : k + 1] * slots + slot)
        here.append(row == at)
    send = (here[0] | here[1]).astype(F32).astype(BF16)
    packed = lax.dot_general(
        send, values[...], (((0,), (0,)), ((), ())), preferred_element_type=F32
    )
    for d in range(chips):
        blocks[d][...] = packed[d * slots : (d + 1) * slots].astype(BF16)
    mix = jnp.where(here[0], meta[:, TOP_K : TOP_K + 1], 0.0) + jnp.where(
        here[1], meta[:, TOP_K + 1 : TOP_K + 2], 0.0
    )
    high = mix.astype(BF16)
    mix_hi[...] = high
    mix_lo[...] = (mix - high.astype(F32)).astype(BF16)


def combine_kernel(mix_hi, mix_lo, *refs):
    blocks, own, other = refs[:-2], refs[-2], refs[-1]
    pieces = jnp.concatenate([b[...].astype(F32) for b in blocks], axis=0).astype(BF16)
    total = jnp.dot(mix_hi[...], pieces, preferred_element_type=F32)
    total = total + jnp.dot(mix_lo[...], pieces, preferred_element_type=F32)
    half = total.shape[0] // CORES
    own[...] = total[:half]
    other[...] = total[half:].astype(BF16)


def expert_rows(rows, slices):
    contract = (((1,), (1,)), ((), ()))
    total = None
    for gate_w, up_w, down_w in slices:
        gate = lax.dot_general(rows, gate_w[...], contract, preferred_element_type=F32)
        upper = lax.dot_general(rows, up_w[...], contract, preferred_element_type=F32)
        hidden = (gate / (1.0 + jnp.exp(-gate)) * upper).astype(BF16)
        part = jnp.dot(hidden, down_w[...], preferred_element_type=F32)
        total = part if total is None else total + part
    return total.astype(BF16)


def ffn_kernel(gate_w, up_w, down_w, pack_a, pack_b, *refs, count):
    third = pack_a.shape[0] // 3
    slices = [(gate_w, up_w, down_w)] + [
        tuple(pack.at[pl.ds(i * third, third)] for i in range(3)) for pack in (pack_a, pack_b)
    ]
    sources, outs = refs[:count], refs[count : 2 * count]
    if count == 1:
        outs[0][...] = expert_rows(sources[0][...], slices)
        return
    taken, made = refs[2 * count :]
    for i in range(count):
        taken[i] = sources[i][...]

    @pl.loop(0, count)
    def _(i):
        made[i] = expert_rows(taken[i], slices)

    for i in range(count):
        outs[i][...] = made[i]


def chunks_of(chips):
    near = sorted(range(chips), key=lambda d: (min(d, chips - d), d))[: chips // 2]
    return [d for d in range(chips) if d not in near], near


def body(tokens, norm_gain, gate_weight, up_weight, down_weight, expert_ids, route_weight):
    tok_rows, width = tokens.shape
    n_tp = lax.axis_size("tp")
    n_ep = lax.axis_size("ep")
    chips = n_ep // CORES
    most = max(2, tok_rows * TOP_K * 5 // (4 * n_ep))
    slots = CORES * most
    ep = lax.axis_index("ep")
    tp = lax.axis_index("tp")
    place = jnp.stack([ep // CORES, ep % CORES]).astype(jnp.int32)

    def swap(values):
        return lax.ppermute(values, "ep", [(i, i ^ 1) for i in range(n_ep)])

    def over_chips(values, d):
        pairs = [(i, (i + CORES * d) % n_ep) for i in range(n_ep)]
        return lax.ppermute(values, "ep", pairs)

    def over_tp(values, step):
        return lax.ppermute(values, "tp", [(i, (i + step) % n_tp) for i in range(n_tp)])

    gate_t = gate_weight[0].T
    up_t = up_weight[0].T
    down = down_weight[0]
    part = gate_t.shape[0] // 2
    weights = (gate_t, up_t, down)
    pack_a = over_tp(jnp.concatenate([w[:part] for w in weights], axis=0), -1)
    pack_b = over_tp(jnp.concatenate([w[part:] for w in weights], axis=0), 1)

    tok_b = swap(tokens)
    own = lambda a: lax.dynamic_slice_in_dim(a.T, tp * tok_rows, tok_rows, 1)
    meta_a = jnp.concatenate(
        [own(expert_ids).astype(F32), own(route_weight), jnp.zeros((8 - 2 * TOP_K, tok_rows), F32)],
        axis=0,
    )
    meta_b = swap(meta_a)
    norm_a = pl.pallas_call(
        norm_kernel,
        in_specs=[VMEM] * 2,
        out_specs=VMEM,
        out_shape=jax.ShapeDtypeStruct(tokens.shape, BF16),
        compiler_params=PARAMS,
        name="norm_own",
    )(tokens, norm_gain[None])
    out_types = [jax.ShapeDtypeStruct((slots, width), BF16)] * chips
    out_types += [jax.ShapeDtypeStruct((CORES * tok_rows, chips * slots), BF16)] * 2
    *blocks, mix_hi, mix_lo = pl.pallas_call(
        functools.partial(dispatch_kernel, chips=chips, slots=slots),
        in_specs=[pl.BlockSpec(memory_space=pltpu.SMEM)] + [VMEM] * 5,
        out_specs=[VMEM] * (chips + 2),
        out_shape=out_types,
        scratch_shapes=[pltpu.VMEM((CORES * tok_rows, width), BF16)],
        compiler_params=PARAMS,
        name="dispatch",
    )(place, norm_a, tok_b, norm_gain[None], meta_a, meta_b)

    def ffn(*sources):
        n = len(sources)
        held = [pltpu.VMEM((n, *sources[0].shape), BF16)] * 2 if n > 1 else []
        return pl.pallas_call(
            functools.partial(ffn_kernel, count=n),
            in_specs=[VMEM] * (5 + n),
            out_specs=[VMEM] * n,
            out_shape=[jax.ShapeDtypeStruct(s.shape, BF16) for s in sources],
            scratch_shapes=held,
            compiler_params=PARAMS,
            name="ffn",
        )(gate_t, up_t, down, pack_a, pack_b, *sources)

    def add(got, part):
        return (got.astype(F32) + part.astype(F32)).astype(BF16)

    half = n_tp // (2 * HOP)
    groups = chunks_of(chips)
    chunks = [
        jnp.concatenate([over_chips(blocks[d], d) if d else blocks[d] for d in group], axis=0)
        for group in groups
    ]
    mine = ffn(*chunks)
    returned = [None] * chips
    for c, (group, way) in enumerate(zip(groups, (HOP, -HOP))):
        fore, back = [chunks[c]], [chunks[c]]
        for s in range(1, half + 1):
            fore.append(over_tp(fore[-1], way))
            if s < half:
                back.append(over_tp(back[-1], -way))
        parts = [None] + [ffn(fore[s], back[s]) for s in range(1, half)]
        (total_fore,) = ffn(fore[half])
        total_back = parts[half - 1][1]
        for h in range(1, half + 1):
            got = over_tp(total_fore, -way)
            total_fore = add(got, parts[half - h][0]) if h < half else got
        for h in range(1, half):
            got = over_tp(total_back, way)
            total_back = add(got, parts[half - 1 - h][1]) if h < half - 1 else got
        pieces = (
            mine[c].astype(F32) + total_fore.astype(F32) + total_back.astype(F32)
        ).astype(BF16)
        for j, d in enumerate(group):
            piece = pieces[j * slots : (j + 1) * slots]
            returned[d] = over_chips(piece, -d) if d else piece

    kept, other = pl.pallas_call(
        combine_kernel,
        in_specs=[VMEM] * (2 + chips),
        out_specs=[VMEM] * 2,
        out_shape=[
            jax.ShapeDtypeStruct((tok_rows, width), F32),
            jax.ShapeDtypeStruct((tok_rows, width), BF16),
        ],
        compiler_params=PARAMS,
        name="combine",
    )(mix_hi, mix_lo, *returned)
    return (kept + swap(other).astype(F32)).astype(BF16)


def solution(mesh):
    placed = (
        P(("grp", "ep", "tp"), None),
        P(),
        P("ep", None, "tp"),
        P("ep", None, "tp"),
        P("ep", "tp", None),
        P(("grp", "ep"), None),
        P(("grp", "ep"), None),
    )
    return jax.shard_map(
        body, mesh=mesh, in_specs=placed, out_specs=P(("grp", "ep", "tp"), None), check_vma=False
    )
```

profile of v0, /device:TPU:513, one launch (start us, length us, event | category | flops | bytes accessed | tf_op | source)
XLA Modules:
  0.0 174.6 jit_solution(12100272893219224091)
XLA Ops:
  0.0 20.4 %collective-permute-start = (bf16[128,1024]{1,0:T(8,128)(2,1)}, bf16[128,1024]{1,0:T(8,128)(2,1)S(1)}, u32[]{:S(2)}, u32[]{:S(2)}) collective-permute-start(bf16[128,1024]{1,0:T(8,128)(2,1)} %tok.1), channel_id=1, source_target_pairs={{0,8},{8,0},{16,24},{24,16},{32,40},{40,32},{48,56},{56,48},{64,72... | collective-permute-start | bytes 786440 | tf_op jit(solution)/shard_map/ppermute | solution.py:124
  20.4 1.2 slice_bitcast_fusion
  21.7 0.2 fusion
  21.8 1.2 pad_maximum_fusion
  23.1 1.2 pad_maximum_fusion.1
  24.2 1.5 collective-permute-start.3
  25.7 0.7 convert_bitcast_fusion
  26.5 1.1 collective-permute-start.1
  27.7 0.2 norm_own.1.norm_a
  27.9 0.6 collective-permute-done.1.meta_b
  28.5 1.7 dispatch.1
  30.3 2.6 %collective-permute-start.9 = (bf16[40,1024]{1,0:T(8,128)(2,1)S(1)}, bf16[40,1024]{1,0:T(8,128)(2,1)S(1)}, u32[]{:S(2)}, u32[]{:S(2)}) collective-permute-start(bf16[40,1024]{1,0:T(8,128)(2,1)S(1)} %get-tuple-element.31), channel_id=1, source_target_pairs={{0,112},{8,120},{16,0},{24,8},{32,16},{40,24},{48,32},{56,40},{64,... | collective-permute-start | bytes 245768 | tf_op jit(solution)/shard_map/ppermute | solution.py:128
  33.0 6.8 %collective-permute-done.4 = bf16[40,1024]{1,0:T(8,128)(2,1)S(1)} collective-permute-done((bf16[40,1024]{1,0:T(8,128)(2,1)S(1)}, bf16[40,1024]{1,0:T(8,128)(2,1)S(1)}, u32[]{:S(2)}, u32[]{:S(2)}) %collective-permute-start.4) | collective-permute-done | bytes 81952 | tf_op jit(solution)/shard_map/ppermute | solution.py:128
  40.0 3.8 %collective-permute-start.6 = (bf16[40,1024]{1,0:T(8,128)(2,1)S(1)}, bf16[40,1024]{1,0:T(8,128)(2,1)S(1)}, u32[]{:S(2)}, u32[]{:S(2)}) collective-permute-start(bf16[40,1024]{1,0:T(8,128)(2,1)S(1)} %get-tuple-element.27), channel_id=1, source_target_pairs={{0,80},{8,88},{16,96},{24,104},{32,112},{40,120},{48,0},{56,8},{64... | collective-permute-start | bytes 245768 | tf_op jit(solution)/shard_map/ppermute | solution.py:128
  43.8 1.4 collective-permute-done.10
  45.2 2.3 %collective-permute-start.7 = (bf16[40,1024]{1,0:T(8,128)(2,1)S(1)}, bf16[40,1024]{1,0:T(8,128)(2,1)S(1)}, u32[]{:S(2)}, u32[]{:S(2)}) collective-permute-start(bf16[40,1024]{1,0:T(8,128)(2,1)S(1)} %get-tuple-element.28), channel_id=1, source_target_pairs={{0,96},{8,104},{16,112},{24,120},{32,0},{40,8},{48,16},{56,24},{64... | collective-permute-start | bytes 245768 | tf_op jit(solution)/shard_map/ppermute | solution.py:128
  47.7 1.6 collective-permute-done.6
  49.3 8.5 %collective-permute-done.7 = bf16[40,1024]{1,0:T(8,128)(2,1)S(1)} collective-permute-done((bf16[40,1024]{1,0:T(8,128)(2,1)S(1)}, bf16[40,1024]{1,0:T(8,128)(2,1)S(1)}, u32[]{:S(2)}, u32[]{:S(2)}) %collective-permute-start.7) | collective-permute-done | bytes 81952 | tf_op jit(solution)/shard_map/ppermute | solution.py:128
  57.8 5.9 %collective-permute-done.11.refs_0_ = bf16[160,1024]{1,0:T(8,128)(2,1)S(1)} collective-permute-done((bf16[160,1024]{1,0:T(8,128)(2,1)S(1)}, bf16[160,1024]{1,0:T(8,128)(2,1)S(1)}, u32[]{:S(2)}, u32[]{:S(2)}) %collective-permute-start.11) | collective-permute-done | bytes 327712 | tf_op jit(solution)/shard_map/ppermute | solution.py:131
  63.7 3.1 %collective-permute-start.12 = (bf16[160,1024]{1,0:T(8,128)(2,1)S(1)}, bf16[160,1024]{1,0:T(8,128)(2,1)S(1)}, u32[]{:S(2)}, u32[]{:S(2)}) collective-permute-start(bf16[160,1024]{1,0:T(8,128)(2,1)S(1)} %collective-permute-done.11.refs_0_), channel_id=1, source_target_pairs={{0,6},{1,7},{2,0},{3,1},{4,2},{5,3},{6,4},{7,5},{8,14},{9,15},{10,... | collective-permute-start | bytes 983048 | tf_op jit(solution)/shard_map/ppermute | solution.py:131
  66.8 9.3 %collective-permute-done.19.refs_0_ = bf16[160,1024]{1,0:T(8,128)(2,1)S(1)} collective-permute-done((bf16[160,1024]{1,0:T(8,128)(2,1)S(1)}, bf16[160,1024]{1,0:T(8,128)(2,1)S(1)}, u32[]{:S(2)}, u32[]{:S(2)}) %collective-permute-start.19) | collective-permute-done | bytes 327712 | tf_op jit(solution)/shard_map/ppermute | solution.py:131
  76.2 1.2 copy-done.5
  77.3 1.9 %ffn.6 = bf16[160,1024]{1,0:T(8,128)(2,1)S(1)} custom-call(bf16[448,1024]{1,0:T(8,128)(2,1)S(1)} %bitcast.19, bf16[448,1024]{1,0:T(8,128)(2,1)S(1)} %bitcast.25, bf16[448,1024]{1,0:T(8,128)(2,1)S(1)} %bitcast.30, bf16[672,1024]{1,0:T(8,128)(2,1)S(1)} %collective-permute-done.2.pack_a, bf16[672,1024]{1,0:T(8,128)(2,1)S(1)} %collective-permute-done.3.pack_b, ...), custom_call_target="tpu_custom_call" | custom-call | tf_op jit(solution)/shard_map/ffn/pallas_call | solution.py:171
  79.2 1.7 collective-permute-start.13
  80.9 2.1 %collective-permute-start.22 = (bf16[160,1024]{1,0:T(8,128)(2,1)S(1)}, bf16[160,1024]{1,0:T(8,128)(2,1)S(1)}, u32[]{:S(2)}, u32[]{:S(2)}) collective-permute-start(bf16[160,1024]{1,0:T(8,128)(2,1)S(1)} %constant_dynamic-update-slice_fusion.refs_0_), channel_id=1, source_target_pairs={{0,6},{1,7},{2,0},{3,1},{4,2},{5,3},{6,4},{7,5},{8,14},{9,15},{10,... | collective-permute-start | bytes 983048 | tf_op jit(solution)/shard_map/ppermute | solution.py:131
  83.1 3.8 %collective-permute-done.20.refs_0_ = bf16[160,1024]{1,0:T(8,128)(2,1)S(1)} collective-permute-done((bf16[160,1024]{1,0:T(8,128)(2,1)S(1)}, bf16[160,1024]{1,0:T(8,128)(2,1)S(1)}, u32[]{:S(2)}, u32[]{:S(2)}) %collective-permute-start.20) | collective-permute-done | bytes 327712 | tf_op jit(solution)/shard_map/ppermute | solution.py:131
  86.8 1.9 %ffn.8 = bf16[160,1024]{1,0:T(8,128)(2,1)S(1)} custom-call(bf16[448,1024]{1,0:T(8,128)(2,1)S(1)} %bitcast.20, bf16[448,1024]{1,0:T(8,128)(2,1)S(1)} %bitcast.26, bf16[448,1024]{1,0:T(8,128)(2,1)S(1)} %bitcast.31, bf16[672,1024]{1,0:T(8,128)(2,1)S(1)} %collective-permute-done.2.pack_a, bf16[672,1024]{1,0:T(8,128)(2,1)S(1)} %collective-permute-done.3.pack_b, ...), custom_call_target="tpu_custom_call" | custom-call | tf_op jit(solution)/shard_map/ffn/pallas_call | solution.py:171
  88.9 5.0 %collective-permute-done.14.refs_1_ = bf16[160,1024]{1,0:T(8,128)(2,1)S(1)} collective-permute-done((bf16[160,1024]{1,0:T(8,128)(2,1)S(1)}, bf16[160,1024]{1,0:T(8,128)(2,1)S(1)}, u32[]{:S(2)}, u32[]{:S(2)}) %collective-permute-start.14) | collective-permute-done | bytes 327712 | tf_op jit(solution)/shard_map/ppermute | solution.py:131
  93.9 3.9 %ffn.7 = (bf16[160,1024]{1,0:T(8,128)(2,1)S(1)}, bf16[160,1024]{1,0:T(8,128)(2,1)S(1)}) custom-call(bf16[448,1024]{1,0:T(8,128)(2,1)S(1)} %bitcast.21, bf16[448,1024]{1,0:T(8,128)(2,1)S(1)} %bitcast.27, bf16[448,1024]{1,0:T(8,128)(2,1)S(1)} %bitcast.32, bf16[672,1024]{1,0:T(8,128)(2,1)S(1)} %collective-permute-done.2.pack_a, ...), custom_call_target="tpu_custom_call" | custom-call | tf_op jit(solution)/shard_map/ffn/pallas_call | solution.py:171
  97.9 24.0 %collective-permute-done.13 = bf16[160,1024]{1,0:T(8,128)(2,1)S(1)} collective-permute-done((bf16[160,1024]{1,0:T(8,128)(2,1)S(1)}, bf16[160,1024]{1,0:T(8,128)(2,1)S(1)}, u32[]{:S(2)}, u32[]{:S(2)}) %collective-permute-start.13) | collective-permute-done | bytes 327712 | tf_op jit(solution)/shard_map/ppermute | solution.py:131
  122.1 3.9 %ffn.9 = (bf16[160,1024]{1,0:T(8,128)(2,1)S(1)}, bf16[160,1024]{1,0:T(8,128)(2,1)S(1)}) custom-call(bf16[448,1024]{1,0:T(8,128)(2,1)S(1)} %bitcast.22, bf16[448,1024]{1,0:T(8,128)(2,1)S(1)} %bitcast.28, bf16[448,1024]{1,0:T(8,128)(2,1)S(1)} %bitcast.33, bf16[672,1024]{1,0:T(8,128)(2,1)S(1)} %collective-permute-done.2.pack_a, ...), custom_call_target="tpu_custom_call" | custom-call | tf_op jit(solution)/shard_map/ffn/pallas_call | solution.py:171
  126.0 0.4 collective-permute-start.24
  126.3 3.8 %ffn.5 = (bf16[160,1024]{1,0:T(8,128)(2,1)S(1)}, bf16[160,1024]{1,0:T(8,128)(2,1)S(1)}) custom-call(bf16[448,1024]{1,0:T(8,128)(2,1)S(1)} %bitcast.23, bf16[448,1024]{1,0:T(8,128)(2,1)S(1)} %bitcast.29, bf16[448,1024]{1,0:T(8,128)(2,1)S(1)} %bitcast.34, bf16[672,1024]{1,0:T(8,128)(2,1)S(1)} %collective-permute-done.2.pack_a, ...), custom_call_target="tpu_custom_call" | custom-call | tf_op jit(solution)/shard_map/ffn/pallas_call | solution.py:171
  130.3 3.7 %collective-permute-start.23 = (bf16[160,1024]{1,0:T(8,128)(2,1)S(1)}, bf16[160,1024]{1,0:T(8,128)(2,1)S(1)}, u32[]{:S(2)}, u32[]{:S(2)}) collective-permute-start(bf16[160,1024]{1,0:T(8,128)(2,1)S(1)} %add_convert_fusion.1), channel_id=1, source_target_pairs={{0,6},{1,7},{2,0},{3,1},{4,2},{5,3},{6,4},{7,5},{8,14},{9,15},{10,... | collective-permute-start | bytes 983048 | tf_op jit(solution)/shard_map/ppermute | solution.py:131
  134.0 0.2 add_convert_fusion.2
  134.2 5.7 %collective-permute-start.17 = (bf16[40,1024]{1,0:T(8,128)(2,1)S(1)}, bf16[40,1024]{1,0:T(8,128)(2,1)S(1)}, u32[]{:S(2)}, u32[]{:S(2)}) collective-permute-start(bf16[40,1024]{1,0:T(8,128)(2,1)S(1)} %get-tuple-element.49), channel_id=1, source_target_pairs={{0,112},{8,120},{16,0},{24,8},{32,16},{40,24},{48,32},{56,40},{64,... | collective-permute-start | bytes 245768 | tf_op jit(solution)/shard_map/ppermute | solution.py:128
  139.9 6.4 %collective-permute-start.18 = (bf16[40,1024]{1,0:T(8,128)(2,1)S(1)}, bf16[40,1024]{1,0:T(8,128)(2,1)S(1)}, u32[]{:S(2)}, u32[]{:S(2)}) collective-permute-start(bf16[40,1024]{1,0:T(8,128)(2,1)S(1)} %get-tuple-element.48), channel_id=1, source_target_pairs={{0,96},{8,104},{16,112},{24,120},{32,0},{40,8},{48,16},{56,24},{64... | collective-permute-start | bytes 245768 | tf_op jit(solution)/shard_map/ppermute | solution.py:128
  146.3 5.7 %collective-permute-done.24 = bf16[160,1024]{1,0:T(8,128)(2,1)S(1)} collective-permute-done((bf16[160,1024]{1,0:T(8,128)(2,1)S(1)}, bf16[160,1024]{1,0:T(8,128)(2,1)S(1)}, u32[]{:S(2)}, u32[]{:S(2)}) %collective-permute-start.24) | collective-permute-done | bytes 327712 | tf_op jit(solution)/shard_map/ppermute | solution.py:131
  151.9 0.2 add_convert_fusion
  152.4 3.1 %collective-permute-start.27 = (bf16[40,1024]{1,0:T(8,128)(2,1)S(1)}, bf16[40,1024]{1,0:T(8,128)(2,1)S(1)}, u32[]{:S(2)}, u32[]{:S(2)}) collective-permute-start(bf16[40,1024]{1,0:T(8,128)(2,1)S(1)} %get-tuple-element.52), channel_id=1, source_target_pairs={{0,48},{8,56},{16,64},{24,72},{32,80},{40,88},{48,96},{56,104},{64... | collective-permute-start | bytes 245768 | tf_op jit(solution)/shard_map/ppermute | solution.py:128
  155.5 2.7 %collective-permute-start.29 = (bf16[40,1024]{1,0:T(8,128)(2,1)S(1)}, bf16[40,1024]{1,0:T(8,128)(2,1)S(1)}, u32[]{:S(2)}, u32[]{:S(2)}) collective-permute-start(bf16[40,1024]{1,0:T(8,128)(2,1)S(1)} %get-tuple-element.47), channel_id=1, source_target_pairs={{0,16},{8,24},{16,32},{24,40},{32,48},{40,56},{48,64},{56,72},{64,... | collective-permute-start | bytes 245768 | tf_op jit(solution)/shard_map/ppermute | solution.py:128
  158.2 4.4 %collective-permute-done.26.refs_4_ = bf16[40,1024]{1,0:T(8,128)(2,1)S(1)} collective-permute-done((bf16[40,1024]{1,0:T(8,128)(2,1)S(1)}, bf16[40,1024]{1,0:T(8,128)(2,1)S(1)}, u32[]{:S(2)}, u32[]{:S(2)}) %collective-permute-start.26) | collective-permute-done | bytes 81952 | tf_op jit(solution)/shard_map/ppermute | solution.py:128
  162.6 0.8 collective-permute-done.28.refs_6_
  163.4 6.8 %collective-permute-done.29.refs_7_ = bf16[40,1024]{1,0:T(8,128)(2,1)S(1)} collective-permute-done((bf16[40,1024]{1,0:T(8,128)(2,1)S(1)}, bf16[40,1024]{1,0:T(8,128)(2,1)S(1)}, u32[]{:S(2)}, u32[]{:S(2)}) %collective-permute-start.29) | collective-permute-done | bytes 81952 | tf_op jit(solution)/shard_map/ppermute | solution.py:128
  170.2 0.7 combine.1
  170.9 1.8 %collective-permute-start.30 = (bf16[128,1024]{1,0:T(8,128)(2,1)S(1)}, bf16[128,1024]{1,0:T(8,128)(2,1)S(1)}, u32[]{:S(2)}, u32[]{:S(2)}) collective-permute-start(bf16[128,1024]{1,0:T(8,128)(2,1)S(1)} %get-tuple-element.40), channel_id=1, source_target_pairs={{0,8},{8,0},{16,24},{24,16},{32,40},{40,32},{48,56},{56,48},{64,72... | collective-permute-start | bytes 786440 | tf_op jit(solution)/shard_map/ppermute | solution.py:124
  172.7 1.2 collective-permute-done.30
  173.8 0.8 add_convert_fusion.4
  (63 shorter events, 1.8 us)
Async XLA Ops:
  0.0 25.7 %copy-start = (f32[1024,2]{0,1:T(2,128)S(1)}, f32[1024,2]{0,1:T(2,128)}, u32[]{:S(2)}) copy-start(f32[1024,2]{0,1:T(2,128)} %param.13) | copy-start | bytes 24580
  0.0 21.6 %copy-start.1 = (bf16[1,1024,448]{1,2,0:T(8,128)(2,1)S(1)}, bf16[1,1024,448]{1,2,0:T(8,128)(2,1)}, u32[]{:S(2)}) copy-start(bf16[1,1024,448]{1,2,0:T(8,128)(2,1)} %param.9) | copy-start | bytes 2752516
  0.0 21.6 %copy-start.3 = (bf16[1,1024,448]{1,2,0:T(8,128)(2,1)S(1)}, bf16[1,1024,448]{1,2,0:T(8,128)(2,1)}, u32[]{:S(2)}) copy-start(bf16[1,1024,448]{1,2,0:T(8,128)(2,1)} %param.10) | copy-start | bytes 2752516
  0.0 28.5 %collective-permute-start = (bf16[128,1024]{1,0:T(8,128)(2,1)}, bf16[128,1024]{1,0:T(8,128)(2,1)S(1)}, u32[]{:S(2)}, u32[]{:S(2)}) collective-permute-start(bf16[128,1024]{1,0:T(8,128)(2,1)} %tok.1), channel_id=1, source_target_pairs={{0,8},{8,0},{16,24},{24,16},{32,40},{40,32},{48,56},{56,48},{64,72... | collective-permute-start | bytes 786440 | tf_op jit(solution)/shard_map/ppermute | solution.py:124
  23.1 53.1 %collective-permute-start.2 = (bf16[672,1024]{1,0:T(8,128)(2,1)}, bf16[672,1024]{1,0:T(8,128)(2,1)S(1)}, u32[]{:S(2)}, u32[]{:S(2)}) collective-permute-start(bf16[672,1024]{1,0:T(8,128)(2,1)} %pad_maximum_fusion), channel_id=1, source_target_pairs={{0,7},{1,0},{2,1},{3,2},{4,3},{5,4},{6,5},{7,6},{8,15},{9,8},{10,9... | collective-permute-start | bytes 4128776 | tf_op jit(solution)/shard_map/ppermute | solution.py:131
  23.1 4.7 %copy-start.6 = (bf16[128,1024]{1,0:T(8,128)(2,1)S(1)}, bf16[128,1024]{1,0:T(8,128)(2,1)}, u32[]{:S(2)}) copy-start(bf16[128,1024]{1,0:T(8,128)(2,1)} %tok.1) | copy-start | bytes 786436
  23.1 4.7 %copy-start.7 = (f32[1024]{0:T(1024)S(1)}, f32[1024]{0:T(1024)}, u32[]{:S(2)}) copy-start(f32[1024]{0:T(1024)} %param.8) | copy-start | bytes 12292
  24.2 51.9 %collective-permute-start.3 = (bf16[672,1024]{1,0:T(8,128)(2,1)}, bf16[672,1024]{1,0:T(8,128)(2,1)S(1)}, u32[]{:S(2)}, u32[]{:S(2)}) collective-permute-start(bf16[672,1024]{1,0:T(8,128)(2,1)} %pad_maximum_fusion.1), channel_id=1, source_target_pairs={{0,1},{1,2},{2,3},{3,4},{4,5},{5,6},{6,7},{7,0},{8,9},{9,10},{10,1... | collective-permute-start | bytes 4128776 | tf_op jit(solution)/shard_map/ppermute | solution.py:131
  26.5 1.9 %collective-permute-start.1 = (f32[8,128]{1,0:T(8,128)S(1)}, f32[8,128]{1,0:T(8,128)S(1)}, u32[]{:S(2)}, u32[]{:S(2)}) collective-permute-start(f32[8,128]{1,0:T(8,128)S(1)} %maximum_maximum_fusion.meta_a), channel_id=1, source_target_pairs={{0,8},{8,0},{16,24},{24,16},{32,40},{40,32},{48,56},{56,48},{64,72... | collective-permute-start | bytes 12296 | tf_op jit(solution)/shard_map/ppermute | solution.py:124
  27.7 48.5 %copy-start.2 = (bf16[1,1024,448]{1,2,0:T(8,128)(2,1)S(1)}, bf16[1,1024,448]{1,2,0:T(8,128)(2,1)}, u32[]{:S(2)}) copy-start(bf16[1,1024,448]{1,2,0:T(8,128)(2,1)} %param.9) | copy-start | bytes 2752516
  27.7 48.5 %copy-start.4 = (bf16[1,1024,448]{1,2,0:T(8,128)(2,1)S(1)}, bf16[1,1024,448]{1,2,0:T(8,128)(2,1)}, u32[]{:S(2)}) copy-start(bf16[1,1024,448]{1,2,0:T(8,128)(2,1)} %param.10) | copy-start | bytes 2752516
  30.2 9.7 %collective-permute-start.8 = (bf16[40,1024]{1,0:T(8,128)(2,1)S(1)}, bf16[40,1024]{1,0:T(8,128)(2,1)S(1)}, u32[]{:S(2)}, u32[]{:S(2)}) collective-permute-start(bf16[40,1024]{1,0:T(8,128)(2,1)S(1)} %get-tuple-element.30), channel_id=1, source_target_pairs={{0,16},{8,24},{16,32},{24,40},{32,48},{40,56},{48,64},{56,72},{64,... | collective-permute-start | bytes 245768 | tf_op jit(solution)/shard_map/ppermute | solution.py:128
  30.3 9.7 %collective-permute-start.9 = (bf16[40,1024]{1,0:T(8,128)(2,1)S(1)}, bf16[40,1024]{1,0:T(8,128)(2,1)S(1)}, u32[]{:S(2)}, u32[]{:S(2)}) collective-permute-start(bf16[40,1024]{1,0:T(8,128)(2,1)S(1)} %get-tuple-element.31), channel_id=1, source_target_pairs={{0,112},{8,120},{16,0},{24,8},{32,16},{40,24},{48,32},{56,40},{64,... | collective-permute-start | bytes 245768 | tf_op jit(solution)/shard_map/ppermute | solution.py:128
  32.9 6.8 %collective-permute-start.4 = (bf16[40,1024]{1,0:T(8,128)(2,1)S(1)}, bf16[40,1024]{1,0:T(8,128)(2,1)S(1)}, u32[]{:S(2)}, u32[]{:S(2)}) collective-permute-start(bf16[40,1024]{1,0:T(8,128)(2,1)S(1)} %get-tuple-element.25), channel_id=1, source_target_pairs={{0,48},{8,56},{16,64},{24,72},{32,80},{40,88},{48,96},{56,104},{64... | collective-permute-start | bytes 245768 | tf_op jit(solution)/shard_map/ppermute | solution.py:128
  39.7 5.5 %collective-permute-start.10 = (bf16[40,1024]{1,0:T(8,128)(2,1)S(1)}, bf16[40,1024]{1,0:T(8,128)(2,1)S(1)}, u32[]{:S(2)}, u32[]{:S(2)}) collective-permute-start(bf16[40,1024]{1,0:T(8,128)(2,1)S(1)} %get-tuple-element.32), channel_id=1, source_target_pairs={{0,32},{8,40},{16,48},{24,56},{32,64},{40,72},{48,80},{56,88},{64,... | collective-permute-start | bytes 245768 | tf_op jit(solution)/shard_map/ppermute | solution.py:128
  39.9 7.7 %collective-permute-start.5 = (bf16[40,1024]{1,0:T(8,128)(2,1)S(1)}, bf16[40,1024]{1,0:T(8,128)(2,1)S(1)}, u32[]{:S(2)}, u32[]{:S(2)}) collective-permute-start(bf16[40,1024]{1,0:T(8,128)(2,1)S(1)} %get-tuple-element.26), channel_id=1, source_target_pairs={{0,64},{8,72},{16,80},{24,88},{32,96},{40,104},{48,112},{56,120},{... | collective-permute-start | bytes 245768 | tf_op jit(solution)/shard_map/ppermute | solution.py:128
  40.0 9.2 %collective-permute-start.6 = (bf16[40,1024]{1,0:T(8,128)(2,1)S(1)}, bf16[40,1024]{1,0:T(8,128)(2,1)S(1)}, u32[]{:S(2)}, u32[]{:S(2)}) collective-permute-start(bf16[40,1024]{1,0:T(8,128)(2,1)S(1)} %get-tuple-element.27), channel_id=1, source_target_pairs={{0,80},{8,88},{16,96},{24,104},{32,112},{40,120},{48,0},{56,8},{64... | collective-permute-start | bytes 245768 | tf_op jit(solution)/shard_map/ppermute | solution.py:128
  45.2 12.5 %collective-permute-start.7 = (bf16[40,1024]{1,0:T(8,128)(2,1)S(1)}, bf16[40,1024]{1,0:T(8,128)(2,1)S(1)}, u32[]{:S(2)}, u32[]{:S(2)}) collective-permute-start(bf16[40,1024]{1,0:T(8,128)(2,1)S(1)} %get-tuple-element.28), channel_id=1, source_target_pairs={{0,96},{8,104},{16,112},{24,120},{32,0},{40,8},{48,16},{56,24},{64... | collective-permute-start | bytes 245768 | tf_op jit(solution)/shard_map/ppermute | solution.py:128
  47.5 16.2 %collective-permute-start.11 = (bf16[160,1024]{1,0:T(8,128)(2,1)S(1)}, bf16[160,1024]{1,0:T(8,128)(2,1)S(1)}, u32[]{:S(2)}, u32[]{:S(2)}) collective-permute-start(bf16[160,1024]{1,0:T(8,128)(2,1)S(1)} %constant_dynamic-update-slice_fusion.4.refs_1_), channel_id=1, source_target_pairs={{0,6},{1,7},{2,0},{3,1},{4,2},{5,3},{6,4},{7,5},{8,14},{9,15},{10,... | collective-permute-start | bytes 983048 | tf_op jit(solution)/shard_map/ppermute | solution.py:131
  57.7 18.4 %collective-permute-start.19 = (bf16[160,1024]{1,0:T(8,128)(2,1)S(1)}, bf16[160,1024]{1,0:T(8,128)(2,1)S(1)}, u32[]{:S(2)}, u32[]{:S(2)}) collective-permute-start(bf16[160,1024]{1,0:T(8,128)(2,1)S(1)} %constant_dynamic-update-slice_fusion.refs_0_), channel_id=1, source_target_pairs={{0,2},{1,3},{2,4},{3,5},{4,6},{5,7},{6,0},{7,1},{8,10},{9,11},{10,... | collective-permute-start | bytes 983048 | tf_op jit(solution)/shard_map/ppermute | solution.py:131
  63.7 12.4 %collective-permute-start.12 = (bf16[160,1024]{1,0:T(8,128)(2,1)S(1)}, bf16[160,1024]{1,0:T(8,128)(2,1)S(1)}, u32[]{:S(2)}, u32[]{:S(2)}) collective-permute-start(bf16[160,1024]{1,0:T(8,128)(2,1)S(1)} %collective-permute-done.11.refs_0_), channel_id=1, source_target_pairs={{0,6},{1,7},{2,0},{3,1},{4,2},{5,3},{6,4},{7,5},{8,14},{9,15},{10,... | collective-permute-start | bytes 983048 | tf_op jit(solution)/shard_map/ppermute | solution.py:131
  76.1 10.7 %collective-permute-start.20 = (bf16[160,1024]{1,0:T(8,128)(2,1)S(1)}, bf16[160,1024]{1,0:T(8,128)(2,1)S(1)}, u32[]{:S(2)}, u32[]{:S(2)}) collective-permute-start(bf16[160,1024]{1,0:T(8,128)(2,1)S(1)} %collective-permute-done.19.refs_0_), channel_id=1, source_target_pairs={{0,2},{1,3},{2,4},{3,5},{4,6},{5,7},{6,0},{7,1},{8,10},{9,11},{10,... | collective-permute-start | bytes 983048 | tf_op jit(solution)/shard_map/ppermute | solution.py:131
  76.1 17.8 %collective-permute-start.14 = (bf16[160,1024]{1,0:T(8,128)(2,1)S(1)}, bf16[160,1024]{1,0:T(8,128)(2,1)S(1)}, u32[]{:S(2)}, u32[]{:S(2)}) collective-permute-start(bf16[160,1024]{1,0:T(8,128)(2,1)S(1)} %constant_dynamic-update-slice_fusion.4.refs_1_), channel_id=1, source_target_pairs={{0,2},{1,3},{2,4},{3,5},{4,6},{5,7},{6,0},{7,1},{8,10},{9,11},{10,... | collective-permute-start | bytes 983048 | tf_op jit(solution)/shard_map/ppermute | solution.py:131
  76.2 1.2 copy-start.5
  79.2 42.6 %collective-permute-start.13 = (bf16[160,1024]{1,0:T(8,128)(2,1)S(1)}, bf16[160,1024]{1,0:T(8,128)(2,1)S(1)}, u32[]{:S(2)}, u32[]{:S(2)}) collective-permute-start(bf16[160,1024]{1,0:T(8,128)(2,1)S(1)} %ffn.6), channel_id=1, source_target_pairs={{0,2},{1,3},{2,4},{3,5},{4,6},{5,7},{6,0},{7,1},{8,10},{9,11},{10,... | collective-permute-start | bytes 983048 | tf_op jit(solution)/shard_map/ppermute | solution.py:131
  80.9 41.2 %collective-permute-start.22 = (bf16[160,1024]{1,0:T(8,128)(2,1)S(1)}, bf16[160,1024]{1,0:T(8,128)(2,1)S(1)}, u32[]{:S(2)}, u32[]{:S(2)}) collective-permute-start(bf16[160,1024]{1,0:T(8,128)(2,1)S(1)} %constant_dynamic-update-slice_fusion.refs_0_), channel_id=1, source_target_pairs={{0,6},{1,7},{2,0},{3,1},{4,2},{5,3},{6,4},{7,5},{8,14},{9,15},{10,... | collective-permute-start | bytes 983048 | tf_op jit(solution)/shard_map/ppermute | solution.py:131
  88.7 41.5 %collective-permute-start.21 = (bf16[160,1024]{1,0:T(8,128)(2,1)S(1)}, bf16[160,1024]{1,0:T(8,128)(2,1)S(1)}, u32[]{:S(2)}, u32[]{:S(2)}) collective-permute-start(bf16[160,1024]{1,0:T(8,128)(2,1)S(1)} %ffn.8), channel_id=1, source_target_pairs={{0,6},{1,7},{2,0},{3,1},{4,2},{5,3},{6,4},{7,5},{8,14},{9,15},{10,... | collective-permute-start | bytes 983048 | tf_op jit(solution)/shard_map/ppermute | solution.py:131
  97.8 36.2 %collective-permute-start.16 = (bf16[160,1024]{1,0:T(8,128)(2,1)S(1)}, bf16[160,1024]{1,0:T(8,128)(2,1)S(1)}, u32[]{:S(2)}, u32[]{:S(2)}) collective-permute-start(bf16[160,1024]{1,0:T(8,128)(2,1)S(1)} %get-tuple-element.35), channel_id=1, source_target_pairs={{0,6},{1,7},{2,0},{3,1},{4,2},{5,3},{6,4},{7,5},{8,14},{9,15},{10,... | collective-permute-start | bytes 983048 | tf_op jit(solution)/shard_map/ppermute | solution.py:131
  122.0 12.0 %collective-permute-start.15 = (bf16[160,1024]{1,0:T(8,128)(2,1)S(1)}, bf16[160,1024]{1,0:T(8,128)(2,1)S(1)}, u32[]{:S(2)}, u32[]{:S(2)}) collective-permute-start(bf16[160,1024]{1,0:T(8,128)(2,1)S(1)} %add_convert_fusion.3), channel_id=1, source_target_pairs={{0,2},{1,3},{2,4},{3,5},{4,6},{5,7},{6,0},{7,1},{8,10},{9,11},{10,... | collective-permute-start | bytes 983048 | tf_op jit(solution)/shard_map/ppermute | solution.py:131
  126.0 26.0 %collective-permute-start.24 = (bf16[160,1024]{1,0:T(8,128)(2,1)S(1)}, bf16[160,1024]{1,0:T(8,128)(2,1)S(1)}, u32[]{:S(2)}, u32[]{:S(2)}) collective-permute-start(bf16[160,1024]{1,0:T(8,128)(2,1)S(1)} %get-tuple-element.38), channel_id=1, source_target_pairs={{0,2},{1,3},{2,4},{3,5},{4,6},{5,7},{6,0},{7,1},{8,10},{9,11},{10,... | collective-permute-start | bytes 983048 | tf_op jit(solution)/shard_map/ppermute | solution.py:131
  130.3 21.6 %collective-permute-start.23 = (bf16[160,1024]{1,0:T(8,128)(2,1)S(1)}, bf16[160,1024]{1,0:T(8,128)(2,1)S(1)}, u32[]{:S(2)}, u32[]{:S(2)}) collective-permute-start(bf16[160,1024]{1,0:T(8,128)(2,1)S(1)} %add_convert_fusion.1), channel_id=1, source_target_pairs={{0,6},{1,7},{2,0},{3,1},{4,2},{5,3},{6,4},{7,5},{8,14},{9,15},{10,... | collective-permute-start | bytes 983048 | tf_op jit(solution)/shard_map/ppermute | solution.py:131
  134.2 21.3 %collective-permute-start.17 = (bf16[40,1024]{1,0:T(8,128)(2,1)S(1)}, bf16[40,1024]{1,0:T(8,128)(2,1)S(1)}, u32[]{:S(2)}, u32[]{:S(2)}) collective-permute-start(bf16[40,1024]{1,0:T(8,128)(2,1)S(1)} %get-tuple-element.49), channel_id=1, source_target_pairs={{0,112},{8,120},{16,0},{24,8},{32,16},{40,24},{48,32},{56,40},{64,... | collective-permute-start | bytes 245768 | tf_op jit(solution)/shard_map/ppermute | solution.py:128
  139.9 15.6 %collective-permute-start.18 = (bf16[40,1024]{1,0:T(8,128)(2,1)S(1)}, bf16[40,1024]{1,0:T(8,128)(2,1)S(1)}, u32[]{:S(2)}, u32[]{:S(2)}) collective-permute-start(bf16[40,1024]{1,0:T(8,128)(2,1)S(1)} %get-tuple-element.48), channel_id=1, source_target_pairs={{0,96},{8,104},{16,112},{24,120},{32,0},{40,8},{48,16},{56,24},{64... | collective-permute-start | bytes 245768 | tf_op jit(solution)/shard_map/ppermute | solution.py:128
  152.1 6.0 %collective-permute-start.25 = (bf16[40,1024]{1,0:T(8,128)(2,1)S(1)}, bf16[40,1024]{1,0:T(8,128)(2,1)S(1)}, u32[]{:S(2)}, u32[]{:S(2)}) collective-permute-start(bf16[40,1024]{1,0:T(8,128)(2,1)S(1)} %get-tuple-element.54), channel_id=1, source_target_pairs={{0,80},{8,88},{16,96},{24,104},{32,112},{40,120},{48,0},{56,8},{64... | collective-permute-start | bytes 245768 | tf_op jit(solution)/shard_map/ppermute | solution.py:128
  152.3 10.3 %collective-permute-start.26 = (bf16[40,1024]{1,0:T(8,128)(2,1)S(1)}, bf16[40,1024]{1,0:T(8,128)(2,1)S(1)}, u32[]{:S(2)}, u32[]{:S(2)}) collective-permute-start(bf16[40,1024]{1,0:T(8,128)(2,1)S(1)} %get-tuple-element.53), channel_id=1, source_target_pairs={{0,64},{8,72},{16,80},{24,88},{32,96},{40,104},{48,112},{56,120},{... | collective-permute-start | bytes 245768 | tf_op jit(solution)/shard_map/ppermute | solution.py:128
  152.4 10.2 %collective-permute-start.27 = (bf16[40,1024]{1,0:T(8,128)(2,1)S(1)}, bf16[40,1024]{1,0:T(8,128)(2,1)S(1)}, u32[]{:S(2)}, u32[]{:S(2)}) collective-permute-start(bf16[40,1024]{1,0:T(8,128)(2,1)S(1)} %get-tuple-element.52), channel_id=1, source_target_pairs={{0,48},{8,56},{16,64},{24,72},{32,80},{40,88},{48,96},{56,104},{64... | collective-permute-start | bytes 245768 | tf_op jit(solution)/shard_map/ppermute | solution.py:128
  155.5 7.9 %collective-permute-start.28 = (bf16[40,1024]{1,0:T(8,128)(2,1)S(1)}, bf16[40,1024]{1,0:T(8,128)(2,1)S(1)}, u32[]{:S(2)}, u32[]{:S(2)}) collective-permute-start(bf16[40,1024]{1,0:T(8,128)(2,1)S(1)} %get-tuple-element.51), channel_id=1, source_target_pairs={{0,32},{8,40},{16,48},{24,56},{32,64},{40,72},{48,80},{56,88},{64,... | collective-permute-start | bytes 245768 | tf_op jit(solution)/shard_map/ppermute | solution.py:128
  155.5 14.6 %collective-permute-start.29 = (bf16[40,1024]{1,0:T(8,128)(2,1)S(1)}, bf16[40,1024]{1,0:T(8,128)(2,1)S(1)}, u32[]{:S(2)}, u32[]{:S(2)}) collective-permute-start(bf16[40,1024]{1,0:T(8,128)(2,1)S(1)} %get-tuple-element.47), channel_id=1, source_target_pairs={{0,16},{8,24},{16,32},{24,40},{32,48},{40,56},{48,64},{56,72},{64,... | collective-permute-start | bytes 245768 | tf_op jit(solution)/shard_map/ppermute | solution.py:128
  170.9 3.0 %collective-permute-start.30 = (bf16[128,1024]{1,0:T(8,128)(2,1)S(1)}, bf16[128,1024]{1,0:T(8,128)(2,1)S(1)}, u32[]{:S(2)}, u32[]{:S(2)}) collective-permute-start(bf16[128,1024]{1,0:T(8,128)(2,1)S(1)} %get-tuple-element.40), channel_id=1, source_target_pairs={{0,8},{8,0},{16,24},{24,16},{32,40},{40,32},{48,56},{56,48},{64,72... | collective-permute-start | bytes 786440 | tf_op jit(solution)/shard_map/ppermute | solution.py:124
where the time goes:
time: 175 us
  waiting for transfers between devices  85.6 us (49%)
  starting transfers between devices  63.5 us (36%)
  Pallas kernels  17.8 us (10%)
  other arithmetic  4.5 us (3%)
  local copies, waits for them, and re-layouts  2.77 us (2%)
    ppermute x14, waiting for transfers between devices, over_tp(): lax.ppermute(values, 'tp', [(i, (i + step) % n_tp) for i in range(n_tp)])  53.7 us
    ppermute x14, waiting for transfers between devices, over_chips(): return lax.ppermute(values, 'ep', pairs)  30.2 us
    ppermute x14, starting transfers between devices, over_chips(): return lax.ppermute(values, 'ep', pairs)  27.3 us
    ppermute x3, starting transfers between devices, swap(): return lax.ppermute(values, 'ep', [(i, i ^ 1) for i in range(n_ep)])  23.3 us
    pallas_call x5, Pallas kernels, ffn(): pl.pallas_call(functools.partial(ffn_kernel, count=n), in_specs=[VMEM] *...  15.3 us
    ppermute x14, starting transfers between devices, over_tp(): lax.ppermute(values, 'tp', [(i, (i + step) % n_tp) for i in range(n_tp)])  13 us
  transfers between devices with their start and end apart: 31, of which 15 were waited for; matrix products, arithmetic and copies ran while one was open for 3% of the time, Pallas kernels for 10%

commit v1 on v0

--- a/solution.py
+++ b/solution.py
@@ -15,6 +15,20 @@
 BF16 = jnp.bfloat16
 VMEM = pl.BlockSpec(memory_space=pltpu.VMEM)
 PARAMS = pltpu.CompilerParams(vmem_limit_bytes=24 * 1024 * 1024)
+
+
+def pack_kernel(gate_w, up_w, down_w, low, high, sems):
+    part = low.shape[0] // 3
+    copies = []
+    for j, out in enumerate((low, high)):
+        for i, weight in enumerate((gate_w, up_w, down_w)):
+            source = weight.at[pl.ds(j * part, part)]
+            target = out.at[pl.ds(i * part, part)]
+            copies.append(pltpu.make_async_copy(source, target, sems.at[3 * j + i]))
+    for copy in copies:
+        copy.start()
+    for copy in copies:
+        copy.wait()
 
 
 def norm_kernel(tok, gain, out):
@@ -71,6 +85,13 @@
     other[...] = total[half:].astype(BF16)
 
 
+def sum_kernel(mine, fore, back, *outs):
+    total = mine[...].astype(F32) + fore[...].astype(F32) + back[...].astype(F32)
+    rows = outs[0].shape[0]
+    for j, out in enumerate(outs):
+        out[...] = total[j * rows : (j + 1) * rows].astype(BF16)
+
+
 def expert_rows(rows, slices):
     contract = (((1,), (1,)), ((), ()))
     total = None
@@ -130,13 +151,24 @@
     def over_tp(values, step):
         return lax.ppermute(values, "tp", [(i, (i + step) % n_tp) for i in range(n_tp)])
 
+    def mirrored(values, step):
+        pairs = [(i, (i + (step if i % HOP else -step)) % n_tp) for i in range(n_tp)]
+        return lax.ppermute(values, "tp", pairs)
+
     gate_t = gate_weight[0].T
     up_t = up_weight[0].T
     down = down_weight[0]
     part = gate_t.shape[0] // 2
-    weights = (gate_t, up_t, down)
-    pack_a = over_tp(jnp.concatenate([w[:part] for w in weights], axis=0), -1)
-    pack_b = over_tp(jnp.concatenate([w[part:] for w in weights], axis=0), 1)
+    low, high = pl.pallas_call(
+        pack_kernel,
+        in_specs=[pl.BlockSpec(memory_space=pltpu.HBM)] * 3,
+        out_specs=[VMEM] * 2,
+        out_shape=[jax.ShapeDtypeStruct((3 * part, width), BF16)] * 2,
+        scratch_shapes=[pltpu.SemaphoreType.DMA((6,))],
+        compiler_params=PARAMS,
+        name="pack",
+    )(gate_t, up_t, down)
+    pack_a, pack_b = over_tp(low, -1), over_tp(high, 1)
 
     tok_b = swap(tokens)
     own = lambda a: lax.dynamic_slice_in_dim(a.T, tp * tok_rows, tok_rows, 1)
@@ -192,23 +224,27 @@
     for c, (group, way) in enumerate(zip(groups, (HOP, -HOP))):
         fore, back = [chunks[c]], [chunks[c]]
         for s in range(1, half + 1):
-            fore.append(over_tp(fore[-1], way))
+            fore.append(mirrored(fore[-1], way))
             if s < half:
-                back.append(over_tp(back[-1], -way))
+                back.append(mirrored(back[-1], -way))
         parts = [None] + [ffn(fore[s], back[s]) for s in range(1, half)]
         (total_fore,) = ffn(fore[half])
         total_back = parts[half - 1][1]
         for h in range(1, half + 1):
-            got = over_tp(total_fore, -way)
+            got = mirrored(total_fore, -way)
             total_fore = add(got, parts[half - h][0]) if h < half else got
         for h in range(1, half):
-            got = over_tp(total_back, way)
+            got = mirrored(total_back, way)
             total_back = add(got, parts[half - 1 - h][1]) if h < half - 1 else got
-        pieces = (
-            mine[c].astype(F32) + total_fore.astype(F32) + total_back.astype(F32)
-        ).astype(BF16)
-        for j, d in enumerate(group):
-            piece = pieces[j * slots : (j + 1) * slots]
+        pieces = pl.pallas_call(
+            sum_kernel,
+            in_specs=[VMEM] * 3,
+            out_specs=[VMEM] * len(group),
+            out_shape=[jax.ShapeDtypeStruct((slots, width), BF16)] * len(group),
+            compiler_params=PARAMS,
+            name="sum_blocks",
+        )(mine[c], total_fore, total_back)
+        for d, piece in zip(group, pieces):
             returned[d] = over_chips(piece, -d) if d else piece
 
     kept, other = pl.pallas_call(

time: 175 us -> 177 us (1.011)
  waiting for transfers between devices: 85.6 us -> 64.8 us
  starting transfers between devices: 63.5 us -> 83.8 us
  Pallas kernels: 17.8 us -> 21.3 us
  other arithmetic: 4.5 us -> 1.78 us
  local copies, waits for them, and re-layouts: 2.77 us -> 4.86 us
    ppermute x14 -> x2, waiting for transfers between devices: 53.7 us -> 0.01 us  [over_tp(): lax.ppermute(values, 'tp', [(i, (i + step) % n_tp) for i in range(n_tp)])]
    ppermute x0 -> x12, waiting for transfers between devices: none -> 38 us  [mirrored(): return lax.ppermute(values, 'tp', pairs)]
    ppermute x0 -> x12, starting transfers between devices: none -> 21.8 us  [mirrored(): return lax.ppermute(values, 'tp', pairs)]
    ppermute x3, starting transfers between devices: 23.3 us -> 34.9 us  [swap(): return lax.ppermute(values, 'ep', [(i, i ^ 1) for i in range(n_ep)])]
    ppermute x14 -> x2, starting transfers between devices: 13 us -> 1.57 us  [over_tp(): lax.ppermute(values, 'tp', [(i, (i + step) % n_tp) for i in range(n_tp)])]
    ppermute x14, waiting for transfers between devices: 30.2 us -> 25.7 us  [over_chips(): return lax.ppermute(values, 'ep', pairs)]
    unnamed x22 -> x24, local copies, waits for them, and re-layouts: 1.24 us -> 4.77 us
    pallas_call x0 -> x3, Pallas kernels: none -> 3.44 us  [the longest x1 3.2 us: body(): pl.pallas_call(pack_kernel, in_specs=[pl.BlockSpec(memory_space=pltpu.HBM...]
  transfers between devices with their start and end apart: 31 -> 31, of which waited for: 15 -> 13; matrix products, arithmetic and copies ran while one was open for 3% -> 1% of each run, Pallas kernels for 10% -> 12%
where the time goes in v1:
time: 177 us
  starting transfers between devices  83.8 us (47%)
  waiting for transfers between devices  64.8 us (37%)
  Pallas kernels  21.3 us (12%)
  local copies, waits for them, and re-layouts  4.86 us (3%)
  other arithmetic  1.78 us (1%)
    ppermute x12, waiting for transfers between devices, mirrored(): return lax.ppermute(values, 'tp', pairs)  38 us
    ppermute x3, starting transfers between devices, swap(): return lax.ppermute(values, 'ep', [(i, i ^ 1) for i in range(n_ep)])  34.9 us
    ppermute x14, waiting for transfers between devices, over_chips(): return lax.ppermute(values, 'ep', pairs)  25.7 us
    ppermute x14, starting transfers between devices, over_chips(): return lax.ppermute(values, 'ep', pairs)  25.5 us
    ppermute x12, starting transfers between devices, mirrored(): return lax.ppermute(values, 'tp', pairs)  21.8 us
    pallas_call x5, Pallas kernels, ffn(): pl.pallas_call(functools.partial(ffn_kernel, count=n), in_specs=[VMEM] *...  15.3 us
    unnamed x24, local copies, waits for them, and re-layouts  4.77 us
  transfers between devices with their start and end apart: 31, of which 13 were waited for; matrix products, arithmetic and copies ran while one was open for 1% of the time, Pallas kernels for 12%

profile of v1, /device:TPU:513, one launch (start us, length us, event | category | flops | bytes accessed | tf_op | source)
XLA Modules:
  0.0 176.8 jit_solution(11054298464056223793)
XLA Ops:
  0.0 20.4 %collective-permute-start = (bf16[128,1024]{1,0:T(8,128)(2,1)}, bf16[128,1024]{1,0:T(8,128)(2,1)S(1)}, u32[]{:S(2)}, u32[]{:S(2)}) collective-permute-start(bf16[128,1024]{1,0:T(8,128)(2,1)} %tok.1), channel_id=1, source_target_pairs={{0,8},{8,0},{16,24},{24,16},{32,40},{40,32},{48,56},{56,48},{64,72... | collective-permute-start | bytes 786440 | tf_op jit(solution)/shard_map/ppermute | solution.py:145
  20.4 0.7 convert_bitcast_fusion
  21.3 0.7 collective-permute-start.1
  22.0 1.2 copy-done.1
  23.2 1.2 copy-done.3
  24.4 1.2 copy-done.5
  25.5 3.2 %pack.1 = (bf16[672,1024]{1,0:T(8,128)(2,1)}, bf16[672,1024]{1,0:T(8,128)(2,1)}) custom-call(bf16[448,1024]{1,0:T(8,128)(2,1)S(1)} %bitcast.14, bf16[448,1024]{1,0:T(8,128)(2,1)S(1)} %bitcast.20, bf16[448,1024]{1,0:T(8,128)(2,1)S(1)} %bitcast.26), custom_call_target="tpu_custom_call" | custom-call | tf_op jit(solution)/shard_map/pack/pallas_call | solution.py:162
  28.9 1.4 collective-permute-start.3
  30.4 0.2 norm_own.1.norm_a
  30.6 1.7 dispatch.1
  32.6 4.3 %collective-permute-start.6 = (bf16[40,1024]{1,0:T(8,128)(2,1)S(1)}, bf16[40,1024]{1,0:T(8,128)(2,1)S(1)}, u32[]{:S(2)}, u32[]{:S(2)}) collective-permute-start(bf16[40,1024]{1,0:T(8,128)(2,1)S(1)} %get-tuple-element.39), channel_id=1, source_target_pairs={{0,80},{8,88},{16,96},{24,104},{32,112},{40,120},{48,0},{56,8},{64... | collective-permute-start | bytes 245768 | tf_op jit(solution)/shard_map/ppermute | solution.py:149
  36.9 2.4 %collective-permute-done.4 = bf16[40,1024]{1,0:T(8,128)(2,1)S(1)} collective-permute-done((bf16[40,1024]{1,0:T(8,128)(2,1)S(1)}, bf16[40,1024]{1,0:T(8,128)(2,1)S(1)}, u32[]{:S(2)}, u32[]{:S(2)}) %collective-permute-start.4) | collective-permute-done | bytes 81952 | tf_op jit(solution)/shard_map/ppermute | solution.py:149
  39.2 4.8 %collective-permute-done.8 = bf16[40,1024]{1,0:T(8,128)(2,1)S(1)} collective-permute-done((bf16[40,1024]{1,0:T(8,128)(2,1)S(1)}, bf16[40,1024]{1,0:T(8,128)(2,1)S(1)}, u32[]{:S(2)}, u32[]{:S(2)}) %collective-permute-start.8) | collective-permute-done | bytes 81952 | tf_op jit(solution)/shard_map/ppermute | solution.py:149
  44.0 3.6 %collective-permute-done.9 = bf16[40,1024]{1,0:T(8,128)(2,1)S(1)} collective-permute-done((bf16[40,1024]{1,0:T(8,128)(2,1)S(1)}, bf16[40,1024]{1,0:T(8,128)(2,1)S(1)}, u32[]{:S(2)}, u32[]{:S(2)}) %collective-permute-start.9) | collective-permute-done | bytes 81952 | tf_op jit(solution)/shard_map/ppermute | solution.py:149
  47.6 5.4 %collective-permute-done.10 = bf16[40,1024]{1,0:T(8,128)(2,1)S(1)} collective-permute-done((bf16[40,1024]{1,0:T(8,128)(2,1)S(1)}, bf16[40,1024]{1,0:T(8,128)(2,1)S(1)}, u32[]{:S(2)}, u32[]{:S(2)}) %collective-permute-start.10) | collective-permute-done | bytes 81952 | tf_op jit(solution)/shard_map/ppermute | solution.py:149
  53.0 0.4 collective-permute-start.7
  53.6 4.0 %collective-permute-done.7 = bf16[40,1024]{1,0:T(8,128)(2,1)S(1)} collective-permute-done((bf16[40,1024]{1,0:T(8,128)(2,1)S(1)}, bf16[40,1024]{1,0:T(8,128)(2,1)S(1)}, u32[]{:S(2)}, u32[]{:S(2)}) %collective-permute-start.7) | collective-permute-done | bytes 81952 | tf_op jit(solution)/shard_map/ppermute | solution.py:149
  57.6 9.1 %collective-permute-done.11.refs_0_ = bf16[160,1024]{1,0:T(8,128)(2,1)S(1)} collective-permute-done((bf16[160,1024]{1,0:T(8,128)(2,1)S(1)}, bf16[160,1024]{1,0:T(8,128)(2,1)S(1)}, u32[]{:S(2)}, u32[]{:S(2)}) %collective-permute-start.11) | collective-permute-done | bytes 327712 | tf_op jit(solution)/shard_map/ppermute | solution.py:156
  66.8 3.2 %collective-permute-start.12 = (bf16[160,1024]{1,0:T(8,128)(2,1)S(1)}, bf16[160,1024]{1,0:T(8,128)(2,1)S(1)}, u32[]{:S(2)}, u32[]{:S(2)}) collective-permute-start(bf16[160,1024]{1,0:T(8,128)(2,1)S(1)} %collective-permute-done.11.refs_0_), channel_id=1, source_target_pairs={{0,2},{1,7},{2,4},{3,1},{4,6},{5,3},{6,0},{7,5},{8,10},{9,15},{10,... | collective-permute-start | bytes 983048 | tf_op jit(solution)/shard_map/ppermute | solution.py:156
  70.0 0.3 collective-permute-start.20
  70.4 8.9 %collective-permute-done.12.refs_0_ = bf16[160,1024]{1,0:T(8,128)(2,1)S(1)} collective-permute-done((bf16[160,1024]{1,0:T(8,128)(2,1)S(1)}, bf16[160,1024]{1,0:T(8,128)(2,1)S(1)}, u32[]{:S(2)}, u32[]{:S(2)}) %collective-permute-start.12) | collective-permute-done | bytes 327712 | tf_op jit(solution)/shard_map/ppermute | solution.py:156
  79.2 3.2 %collective-permute-start.22 = (bf16[160,1024]{1,0:T(8,128)(2,1)S(1)}, bf16[160,1024]{1,0:T(8,128)(2,1)S(1)}, u32[]{:S(2)}, u32[]{:S(2)}) collective-permute-start(bf16[160,1024]{1,0:T(8,128)(2,1)S(1)} %constant_dynamic-update-slice_fusion.refs_0_), channel_id=1, source_target_pairs={{0,2},{1,7},{2,4},{3,1},{4,6},{5,3},{6,0},{7,5},{8,10},{9,15},{10,... | collective-permute-start | bytes 983048 | tf_op jit(solution)/shard_map/ppermute | solution.py:156
  82.4 1.2 copy-done.6
  83.6 1.9 %ffn.6 = bf16[160,1024]{1,0:T(8,128)(2,1)S(1)} custom-call(bf16[448,1024]{1,0:T(8,128)(2,1)S(1)} %bitcast.15, bf16[448,1024]{1,0:T(8,128)(2,1)S(1)} %bitcast.21, bf16[448,1024]{1,0:T(8,128)(2,1)S(1)} %bitcast.27, bf16[672,1024]{1,0:T(8,128)(2,1)S(1)} %collective-permute-done.2.pack_a, bf16[672,1024]{1,0:T(8,128)(2,1)S(1)} %collective-permute-done.3.pack_b, ...), custom_call_target="tpu_custom_call" | custom-call | tf_op jit(solution)/shard_map/ffn/pallas_call | solution.py:203
  85.5 0.5 collective-permute-start.13
  86.0 1.9 %ffn.8 = bf16[160,1024]{1,0:T(8,128)(2,1)S(1)} custom-call(bf16[448,1024]{1,0:T(8,128)(2,1)S(1)} %bitcast.16, bf16[448,1024]{1,0:T(8,128)(2,1)S(1)} %bitcast.22, bf16[448,1024]{1,0:T(8,128)(2,1)S(1)} %bitcast.28, bf16[672,1024]{1,0:T(8,128)(2,1)S(1)} %collective-permute-done.2.pack_a, bf16[672,1024]{1,0:T(8,128)(2,1)S(1)} %collective-permute-done.3.pack_b, ...), custom_call_target="tpu_custom_call" | custom-call | tf_op jit(solution)/shard_map/ffn/pallas_call | solution.py:203
  87.9 4.0 %collective-permute-start.21 = (bf16[160,1024]{1,0:T(8,128)(2,1)S(1)}, bf16[160,1024]{1,0:T(8,128)(2,1)S(1)}, u32[]{:S(2)}, u32[]{:S(2)}) collective-permute-start(bf16[160,1024]{1,0:T(8,128)(2,1)S(1)} %ffn.8), channel_id=1, source_target_pairs={{0,2},{1,7},{2,4},{3,1},{4,6},{5,3},{6,0},{7,5},{8,10},{9,15},{10,... | collective-permute-start | bytes 983048 | tf_op jit(solution)/shard_map/ppermute | solution.py:156
  91.9 3.9 %ffn.7 = (bf16[160,1024]{1,0:T(8,128)(2,1)S(1)}, bf16[160,1024]{1,0:T(8,128)(2,1)S(1)}) custom-call(bf16[448,1024]{1,0:T(8,128)(2,1)S(1)} %bitcast.17, bf16[448,1024]{1,0:T(8,128)(2,1)S(1)} %bitcast.23, bf16[448,1024]{1,0:T(8,128)(2,1)S(1)} %bitcast.29, bf16[672,1024]{1,0:T(8,128)(2,1)S(1)} %collective-permute-done.2.pack_a, ...), custom_call_target="tpu_custom_call" | custom-call | tf_op jit(solution)/shard_map/ffn/pallas_call | solution.py:203
  95.8 3.7 %collective-permute-start.16 = (bf16[160,1024]{1,0:T(8,128)(2,1)S(1)}, bf16[160,1024]{1,0:T(8,128)(2,1)S(1)}, u32[]{:S(2)}, u32[]{:S(2)}) collective-permute-start(bf16[160,1024]{1,0:T(8,128)(2,1)S(1)} %get-tuple-element.47), channel_id=1, source_target_pairs={{0,2},{1,7},{2,4},{3,1},{4,6},{5,3},{6,0},{7,5},{8,10},{9,15},{10,... | collective-permute-start | bytes 983048 | tf_op jit(solution)/shard_map/ppermute | solution.py:156
  99.5 5.7 %collective-permute-done.22.refs_1_ = bf16[160,1024]{1,0:T(8,128)(2,1)S(1)} collective-permute-done((bf16[160,1024]{1,0:T(8,128)(2,1)S(1)}, bf16[160,1024]{1,0:T(8,128)(2,1)S(1)}, u32[]{:S(2)}, u32[]{:S(2)}) %collective-permute-start.22) | collective-permute-done | bytes 327712 | tf_op jit(solution)/shard_map/ppermute | solution.py:156
  105.1 3.8 %ffn.9 = (bf16[160,1024]{1,0:T(8,128)(2,1)S(1)}, bf16[160,1024]{1,0:T(8,128)(2,1)S(1)}) custom-call(bf16[448,1024]{1,0:T(8,128)(2,1)S(1)} %bitcast.18, bf16[448,1024]{1,0:T(8,128)(2,1)S(1)} %bitcast.24, bf16[448,1024]{1,0:T(8,128)(2,1)S(1)} %bitcast.30, bf16[672,1024]{1,0:T(8,128)(2,1)S(1)} %collective-permute-done.2.pack_a, ...), custom_call_target="tpu_custom_call" | custom-call | tf_op jit(solution)/shard_map/ffn/pallas_call | solution.py:203
  109.0 1.5 collective-permute-start.24
  110.6 4.8 %collective-permute-start.15 = (bf16[160,1024]{1,0:T(8,128)(2,1)S(1)}, bf16[160,1024]{1,0:T(8,128)(2,1)S(1)}, u32[]{:S(2)}, u32[]{:S(2)}) collective-permute-start(bf16[160,1024]{1,0:T(8,128)(2,1)S(1)} %add_convert_fusion.1), channel_id=1, source_target_pairs={{0,6},{1,3},{2,0},{3,5},{4,2},{5,7},{6,4},{7,1},{8,14},{9,11},{10,... | collective-permute-start | bytes 983048 | tf_op jit(solution)/shard_map/ppermute | solution.py:156
  115.5 0.4 collective-permute-start.23
  115.9 3.9 %ffn.5 = (bf16[160,1024]{1,0:T(8,128)(2,1)S(1)}, bf16[160,1024]{1,0:T(8,128)(2,1)S(1)}) custom-call(bf16[448,1024]{1,0:T(8,128)(2,1)S(1)} %bitcast.19, bf16[448,1024]{1,0:T(8,128)(2,1)S(1)} %bitcast.25, bf16[448,1024]{1,0:T(8,128)(2,1)S(1)} %bitcast.31, bf16[672,1024]{1,0:T(8,128)(2,1)S(1)} %collective-permute-done.2.pack_a, ...), custom_call_target="tpu_custom_call" | custom-call | tf_op jit(solution)/shard_map/ffn/pallas_call | solution.py:203
  119.8 14.3 %collective-permute-done.15.fore = bf16[160,1024]{1,0:T(8,128)(2,1)S(1)} collective-permute-done((bf16[160,1024]{1,0:T(8,128)(2,1)S(1)}, bf16[160,1024]{1,0:T(8,128)(2,1)S(1)}, u32[]{:S(2)}, u32[]{:S(2)}) %collective-permute-start.15) | collective-permute-done | bytes 327712 | tf_op jit(solution)/shard_map/ppermute | solution.py:156
  134.2 2.6 %collective-permute-start.17 = (bf16[40,1024]{1,0:T(8,128)(2,1)S(1)}, bf16[40,1024]{1,0:T(8,128)(2,1)S(1)}, u32[]{:S(2)}, u32[]{:S(2)}) collective-permute-start(bf16[40,1024]{1,0:T(8,128)(2,1)S(1)} %get-tuple-element.49), channel_id=1, source_target_pairs={{0,112},{8,120},{16,0},{24,8},{32,16},{40,24},{48,32},{56,40},{64,... | collective-permute-start | bytes 245768 | tf_op jit(solution)/shard_map/ppermute | solution.py:149
  136.7 10.0 %collective-permute-start.18 = (bf16[40,1024]{1,0:T(8,128)(2,1)S(1)}, bf16[40,1024]{1,0:T(8,128)(2,1)S(1)}, u32[]{:S(2)}, u32[]{:S(2)}) collective-permute-start(bf16[40,1024]{1,0:T(8,128)(2,1)S(1)} %get-tuple-element.50), channel_id=1, source_target_pairs={{0,96},{8,104},{16,112},{24,120},{32,0},{40,8},{48,16},{56,24},{64... | collective-permute-start | bytes 245768 | tf_op jit(solution)/shard_map/ppermute | solution.py:149
  147.0 5.5 %collective-permute-start.26 = (bf16[40,1024]{1,0:T(8,128)(2,1)S(1)}, bf16[40,1024]{1,0:T(8,128)(2,1)S(1)}, u32[]{:S(2)}, u32[]{:S(2)}) collective-permute-start(bf16[40,1024]{1,0:T(8,128)(2,1)S(1)} %get-tuple-element.55), channel_id=1, source_target_pairs={{0,64},{8,72},{16,80},{24,88},{32,96},{40,104},{48,112},{56,120},{... | collective-permute-start | bytes 245768 | tf_op jit(solution)/shard_map/ppermute | solution.py:149
  152.5 1.3 collective-permute-start.28
  153.8 1.0 collective-permute-start.29
  154.9 0.3 collective-permute-done.26.refs_4_
  155.1 4.2 %collective-permute-done.27.refs_5_ = bf16[40,1024]{1,0:T(8,128)(2,1)S(1)} collective-permute-done((bf16[40,1024]{1,0:T(8,128)(2,1)S(1)}, bf16[40,1024]{1,0:T(8,128)(2,1)S(1)}, u32[]{:S(2)}, u32[]{:S(2)}) %collective-permute-start.27) | collective-permute-done | bytes 81952 | tf_op jit(solution)/shard_map/ppermute | solution.py:149
  159.4 1.1 collective-permute-done.29.refs_7_
  160.5 0.7 combine.1
  161.2 13.7 %collective-permute-start.30 = (bf16[128,1024]{1,0:T(8,128)(2,1)S(1)}, bf16[128,1024]{1,0:T(8,128)(2,1)S(1)}, u32[]{:S(2)}, u32[]{:S(2)}) collective-permute-start(bf16[128,1024]{1,0:T(8,128)(2,1)S(1)} %get-tuple-element.60), channel_id=1, source_target_pairs={{0,8},{8,0},{16,24},{24,16},{32,40},{40,32},{48,56},{56,48},{64,72... | collective-permute-start | bytes 786440 | tf_op jit(solution)/shard_map/ppermute | solution.py:145
  174.9 1.2 collective-permute-done.30
  176.1 0.8 add_convert_fusion.2
  (60 shorter events, 1.5 us)
Async XLA Ops:
  0.0 20.4 %copy-start = (f32[1024,2]{0,1:T(2,128)S(1)}, f32[1024,2]{0,1:T(2,128)}, u32[]{:S(2)}) copy-start(f32[1024,2]{0,1:T(2,128)} %param.13) | copy-start | bytes 24580
  0.0 30.6 %collective-permute-start = (bf16[128,1024]{1,0:T(8,128)(2,1)}, bf16[128,1024]{1,0:T(8,128)(2,1)S(1)}, u32[]{:S(2)}, u32[]{:S(2)}) collective-permute-start(bf16[128,1024]{1,0:T(8,128)(2,1)} %tok.1), channel_id=1, source_target_pairs={{0,8},{8,0},{16,24},{24,16},{32,40},{40,32},{48,56},{56,48},{64,72... | collective-permute-start | bytes 786440 | tf_op jit(solution)/shard_map/ppermute | solution.py:145
  21.3 9.3 %collective-permute-start.1 = (f32[8,128]{1,0:T(8,128)S(1)}, f32[8,128]{1,0:T(8,128)S(1)}, u32[]{:S(2)}, u32[]{:S(2)}) collective-permute-start(f32[8,128]{1,0:T(8,128)S(1)} %maximum_maximum_fusion.meta_a), channel_id=1, source_target_pairs={{0,8},{8,0},{16,24},{24,16},{32,40},{40,32},{48,56},{56,48},{64,72... | collective-permute-start | bytes 12296 | tf_op jit(solution)/shard_map/ppermute | solution.py:145
  22.0 1.2 copy-start.1
  23.2 1.2 copy-start.3
  24.4 1.2 copy-start.5
  25.5 4.9 %copy-start.7 = (bf16[128,1024]{1,0:T(8,128)(2,1)S(1)}, bf16[128,1024]{1,0:T(8,128)(2,1)}, u32[]{:S(2)}) copy-start(bf16[128,1024]{1,0:T(8,128)(2,1)} %tok.1) | copy-start | bytes 786436
  25.5 4.9 %copy-start.8 = (f32[1024]{0:T(1024)S(1)}, f32[1024]{0:T(1024)}, u32[]{:S(2)}) copy-start(f32[1024]{0:T(1024)} %param.8) | copy-start | bytes 12292
  28.8 53.6 %collective-permute-start.2 = (bf16[672,1024]{1,0:T(8,128)(2,1)}, bf16[672,1024]{1,0:T(8,128)(2,1)S(1)}, u32[]{:S(2)}, u32[]{:S(2)}) collective-permute-start(bf16[672,1024]{1,0:T(8,128)(2,1)} %get-tuple-element.35), channel_id=1, source_target_pairs={{0,7},{1,0},{2,1},{3,2},{4,3},{5,4},{6,5},{7,6},{8,15},{9,8},{10,9... | collective-permute-start | bytes 4128776 | tf_op jit(solution)/shard_map/ppermute | solution.py:152
  28.9 53.5 %collective-permute-start.3 = (bf16[672,1024]{1,0:T(8,128)(2,1)}, bf16[672,1024]{1,0:T(8,128)(2,1)S(1)}, u32[]{:S(2)}, u32[]{:S(2)}) collective-permute-start(bf16[672,1024]{1,0:T(8,128)(2,1)} %get-tuple-element.36), channel_id=1, source_target_pairs={{0,1},{1,2},{2,3},{3,4},{4,5},{5,6},{6,7},{7,0},{8,9},{9,10},{10,1... | collective-permute-start | bytes 4128776 | tf_op jit(solution)/shard_map/ppermute | solution.py:152
  30.3 52.1 %copy-start.2 = (bf16[1,1024,448]{1,2,0:T(8,128)(2,1)S(1)}, bf16[1,1024,448]{1,2,0:T(8,128)(2,1)}, u32[]{:S(2)}) copy-start(bf16[1,1024,448]{1,2,0:T(8,128)(2,1)} %param.9) | copy-start | bytes 2752516
  30.3 52.1 %copy-start.4 = (bf16[1,1024,448]{1,2,0:T(8,128)(2,1)S(1)}, bf16[1,1024,448]{1,2,0:T(8,128)(2,1)}, u32[]{:S(2)}) copy-start(bf16[1,1024,448]{1,2,0:T(8,128)(2,1)} %param.10) | copy-start | bytes 2752516
  32.3 7.0 %collective-permute-start.4 = (bf16[40,1024]{1,0:T(8,128)(2,1)S(1)}, bf16[40,1024]{1,0:T(8,128)(2,1)S(1)}, u32[]{:S(2)}, u32[]{:S(2)}) collective-permute-start(bf16[40,1024]{1,0:T(8,128)(2,1)S(1)} %get-tuple-element.37), channel_id=1, source_target_pairs={{0,48},{8,56},{16,64},{24,72},{32,80},{40,88},{48,96},{56,104},{64... | collective-permute-start | bytes 245768 | tf_op jit(solution)/shard_map/ppermute | solution.py:149
  32.4 21.0 %collective-permute-start.5 = (bf16[40,1024]{1,0:T(8,128)(2,1)S(1)}, bf16[40,1024]{1,0:T(8,128)(2,1)S(1)}, u32[]{:S(2)}, u32[]{:S(2)}) collective-permute-start(bf16[40,1024]{1,0:T(8,128)(2,1)S(1)} %get-tuple-element.38), channel_id=1, source_target_pairs={{0,64},{8,72},{16,80},{24,88},{32,96},{40,104},{48,112},{56,120},{... | collective-permute-start | bytes 245768 | tf_op jit(solution)/shard_map/ppermute | solution.py:149
  32.6 21.0 %collective-permute-start.6 = (bf16[40,1024]{1,0:T(8,128)(2,1)S(1)}, bf16[40,1024]{1,0:T(8,128)(2,1)S(1)}, u32[]{:S(2)}, u32[]{:S(2)}) collective-permute-start(bf16[40,1024]{1,0:T(8,128)(2,1)S(1)} %get-tuple-element.39), channel_id=1, source_target_pairs={{0,80},{8,88},{16,96},{24,104},{32,112},{40,120},{48,0},{56,8},{64... | collective-permute-start | bytes 245768 | tf_op jit(solution)/shard_map/ppermute | solution.py:149
  39.2 4.8 %collective-permute-start.8 = (bf16[40,1024]{1,0:T(8,128)(2,1)S(1)}, bf16[40,1024]{1,0:T(8,128)(2,1)S(1)}, u32[]{:S(2)}, u32[]{:S(2)}) collective-permute-start(bf16[40,1024]{1,0:T(8,128)(2,1)S(1)} %get-tuple-element.42), channel_id=1, source_target_pairs={{0,16},{8,24},{16,32},{24,40},{32,48},{40,56},{48,64},{56,72},{64,... | collective-permute-start | bytes 245768 | tf_op jit(solution)/shard_map/ppermute | solution.py:149
  44.0 3.6 %collective-permute-start.9 = (bf16[40,1024]{1,0:T(8,128)(2,1)S(1)}, bf16[40,1024]{1,0:T(8,128)(2,1)S(1)}, u32[]{:S(2)}, u32[]{:S(2)}) collective-permute-start(bf16[40,1024]{1,0:T(8,128)(2,1)S(1)} %get-tuple-element.43), channel_id=1, source_target_pairs={{0,112},{8,120},{16,0},{24,8},{32,16},{40,24},{48,32},{56,40},{64,... | collective-permute-start | bytes 245768 | tf_op jit(solution)/shard_map/ppermute | solution.py:149
  47.6 5.4 %collective-permute-start.10 = (bf16[40,1024]{1,0:T(8,128)(2,1)S(1)}, bf16[40,1024]{1,0:T(8,128)(2,1)S(1)}, u32[]{:S(2)}, u32[]{:S(2)}) collective-permute-start(bf16[40,1024]{1,0:T(8,128)(2,1)S(1)} %get-tuple-element.44), channel_id=1, source_target_pairs={{0,32},{8,40},{16,48},{24,56},{32,64},{40,72},{48,80},{56,88},{64,... | collective-permute-start | bytes 245768 | tf_op jit(solution)/shard_map/ppermute | solution.py:149
  53.0 4.6 %collective-permute-start.7 = (bf16[40,1024]{1,0:T(8,128)(2,1)S(1)}, bf16[40,1024]{1,0:T(8,128)(2,1)S(1)}, u32[]{:S(2)}, u32[]{:S(2)}) collective-permute-start(bf16[40,1024]{1,0:T(8,128)(2,1)S(1)} %get-tuple-element.40), channel_id=1, source_target_pairs={{0,96},{8,104},{16,112},{24,120},{32,0},{40,8},{48,16},{56,24},{64... | collective-permute-start | bytes 245768 | tf_op jit(solution)/shard_map/ppermute | solution.py:149
  53.4 13.3 %collective-permute-start.11 = (bf16[160,1024]{1,0:T(8,128)(2,1)S(1)}, bf16[160,1024]{1,0:T(8,128)(2,1)S(1)}, u32[]{:S(2)}, u32[]{:S(2)}) collective-permute-start(bf16[160,1024]{1,0:T(8,128)(2,1)S(1)} %constant_dynamic-update-slice_fusion.4.refs_1_), channel_id=1, source_target_pairs={{0,2},{1,7},{2,4},{3,1},{4,6},{5,3},{6,0},{7,5},{8,10},{9,15},{10,... | collective-permute-start | bytes 983048 | tf_op jit(solution)/shard_map/ppermute | solution.py:156
  57.6 12.4 %collective-permute-start.19 = (bf16[160,1024]{1,0:T(8,128)(2,1)S(1)}, bf16[160,1024]{1,0:T(8,128)(2,1)S(1)}, u32[]{:S(2)}, u32[]{:S(2)}) collective-permute-start(bf16[160,1024]{1,0:T(8,128)(2,1)S(1)} %constant_dynamic-update-slice_fusion.refs_0_), channel_id=1, source_target_pairs={{0,6},{1,3},{2,0},{3,5},{4,2},{5,7},{6,4},{7,1},{8,14},{9,11},{10,... | collective-permute-start | bytes 983048 | tf_op jit(solution)/shard_map/ppermute | solution.py:156
  66.8 12.5 %collective-permute-start.12 = (bf16[160,1024]{1,0:T(8,128)(2,1)S(1)}, bf16[160,1024]{1,0:T(8,128)(2,1)S(1)}, u32[]{:S(2)}, u32[]{:S(2)}) collective-permute-start(bf16[160,1024]{1,0:T(8,128)(2,1)S(1)} %collective-permute-done.11.refs_0_), channel_id=1, source_target_pairs={{0,2},{1,7},{2,4},{3,1},{4,6},{5,3},{6,0},{7,5},{8,10},{9,15},{10,... | collective-permute-start | bytes 983048 | tf_op jit(solution)/shard_map/ppermute | solution.py:156
  70.0 16.0 %collective-permute-start.20 = (bf16[160,1024]{1,0:T(8,128)(2,1)S(1)}, bf16[160,1024]{1,0:T(8,128)(2,1)S(1)}, u32[]{:S(2)}, u32[]{:S(2)}) collective-permute-start(bf16[160,1024]{1,0:T(8,128)(2,1)S(1)} %collective-permute-done.19.refs_0_), channel_id=1, source_target_pairs={{0,6},{1,3},{2,0},{3,5},{4,2},{5,7},{6,4},{7,1},{8,14},{9,11},{10,... | collective-permute-start | bytes 983048 | tf_op jit(solution)/shard_map/ppermute | solution.py:156
  70.3 21.6 %collective-permute-start.14 = (bf16[160,1024]{1,0:T(8,128)(2,1)S(1)}, bf16[160,1024]{1,0:T(8,128)(2,1)S(1)}, u32[]{:S(2)}, u32[]{:S(2)}) collective-permute-start(bf16[160,1024]{1,0:T(8,128)(2,1)S(1)} %constant_dynamic-update-slice_fusion.4.refs_1_), channel_id=1, source_target_pairs={{0,6},{1,3},{2,0},{3,5},{4,2},{5,7},{6,4},{7,1},{8,14},{9,11},{10,... | collective-permute-start | bytes 983048 | tf_op jit(solution)/shard_map/ppermute | solution.py:156
  79.2 25.9 %collective-permute-start.22 = (bf16[160,1024]{1,0:T(8,128)(2,1)S(1)}, bf16[160,1024]{1,0:T(8,128)(2,1)S(1)}, u32[]{:S(2)}, u32[]{:S(2)}) collective-permute-start(bf16[160,1024]{1,0:T(8,128)(2,1)S(1)} %constant_dynamic-update-slice_fusion.refs_0_), channel_id=1, source_target_pairs={{0,2},{1,7},{2,4},{3,1},{4,6},{5,3},{6,0},{7,5},{8,10},{9,15},{10,... | collective-permute-start | bytes 983048 | tf_op jit(solution)/shard_map/ppermute | solution.py:156
  82.4 1.2 copy-start.6
  85.5 25.0 %collective-permute-start.13 = (bf16[160,1024]{1,0:T(8,128)(2,1)S(1)}, bf16[160,1024]{1,0:T(8,128)(2,1)S(1)}, u32[]{:S(2)}, u32[]{:S(2)}) collective-permute-start(bf16[160,1024]{1,0:T(8,128)(2,1)S(1)} %ffn.6), channel_id=1, source_target_pairs={{0,6},{1,3},{2,0},{3,5},{4,2},{5,7},{6,4},{7,1},{8,14},{9,11},{10,... | collective-permute-start | bytes 983048 | tf_op jit(solution)/shard_map/ppermute | solution.py:156
  87.9 27.5 %collective-permute-start.21 = (bf16[160,1024]{1,0:T(8,128)(2,1)S(1)}, bf16[160,1024]{1,0:T(8,128)(2,1)S(1)}, u32[]{:S(2)}, u32[]{:S(2)}) collective-permute-start(bf16[160,1024]{1,0:T(8,128)(2,1)S(1)} %ffn.8), channel_id=1, source_target_pairs={{0,2},{1,7},{2,4},{3,1},{4,6},{5,3},{6,0},{7,5},{8,10},{9,15},{10,... | collective-permute-start | bytes 983048 | tf_op jit(solution)/shard_map/ppermute | solution.py:156
  95.8 23.9 %collective-permute-start.16 = (bf16[160,1024]{1,0:T(8,128)(2,1)S(1)}, bf16[160,1024]{1,0:T(8,128)(2,1)S(1)}, u32[]{:S(2)}, u32[]{:S(2)}) collective-permute-start(bf16[160,1024]{1,0:T(8,128)(2,1)S(1)} %get-tuple-element.47), channel_id=1, source_target_pairs={{0,2},{1,7},{2,4},{3,1},{4,6},{5,3},{6,0},{7,5},{8,10},{9,15},{10,... | collective-permute-start | bytes 983048 | tf_op jit(solution)/shard_map/ppermute | solution.py:156
  109.0 37.7 %collective-permute-start.24 = (bf16[160,1024]{1,0:T(8,128)(2,1)S(1)}, bf16[160,1024]{1,0:T(8,128)(2,1)S(1)}, u32[]{:S(2)}, u32[]{:S(2)}) collective-permute-start(bf16[160,1024]{1,0:T(8,128)(2,1)S(1)} %get-tuple-element.53), channel_id=1, source_target_pairs={{0,6},{1,3},{2,0},{3,5},{4,2},{5,7},{6,4},{7,1},{8,14},{9,11},{10,... | collective-permute-start | bytes 983048 | tf_op jit(solution)/shard_map/ppermute | solution.py:156
  110.6 23.4 %collective-permute-start.15 = (bf16[160,1024]{1,0:T(8,128)(2,1)S(1)}, bf16[160,1024]{1,0:T(8,128)(2,1)S(1)}, u32[]{:S(2)}, u32[]{:S(2)}) collective-permute-start(bf16[160,1024]{1,0:T(8,128)(2,1)S(1)} %add_convert_fusion.1), channel_id=1, source_target_pairs={{0,6},{1,3},{2,0},{3,5},{4,2},{5,7},{6,4},{7,1},{8,14},{9,11},{10,... | collective-permute-start | bytes 983048 | tf_op jit(solution)/shard_map/ppermute | solution.py:156
  115.5 31.2 %collective-permute-start.23 = (bf16[160,1024]{1,0:T(8,128)(2,1)S(1)}, bf16[160,1024]{1,0:T(8,128)(2,1)S(1)}, u32[]{:S(2)}, u32[]{:S(2)}) collective-permute-start(bf16[160,1024]{1,0:T(8,128)(2,1)S(1)} %add_convert_fusion), channel_id=1, source_target_pairs={{0,2},{1,7},{2,4},{3,1},{4,6},{5,3},{6,0},{7,5},{8,10},{9,15},{10,... | collective-permute-start | bytes 983048 | tf_op jit(solution)/shard_map/ppermute | solution.py:156
  134.2 18.3 %collective-permute-start.17 = (bf16[40,1024]{1,0:T(8,128)(2,1)S(1)}, bf16[40,1024]{1,0:T(8,128)(2,1)S(1)}, u32[]{:S(2)}, u32[]{:S(2)}) collective-permute-start(bf16[40,1024]{1,0:T(8,128)(2,1)S(1)} %get-tuple-element.49), channel_id=1, source_target_pairs={{0,112},{8,120},{16,0},{24,8},{32,16},{40,24},{48,32},{56,40},{64,... | collective-permute-start | bytes 245768 | tf_op jit(solution)/shard_map/ppermute | solution.py:149
  136.7 17.1 %collective-permute-start.18 = (bf16[40,1024]{1,0:T(8,128)(2,1)S(1)}, bf16[40,1024]{1,0:T(8,128)(2,1)S(1)}, u32[]{:S(2)}, u32[]{:S(2)}) collective-permute-start(bf16[40,1024]{1,0:T(8,128)(2,1)S(1)} %get-tuple-element.50), channel_id=1, source_target_pairs={{0,96},{8,104},{16,112},{24,120},{32,0},{40,8},{48,16},{56,24},{64... | collective-permute-start | bytes 245768 | tf_op jit(solution)/shard_map/ppermute | solution.py:149
  146.8 8.0 %collective-permute-start.25 = (bf16[40,1024]{1,0:T(8,128)(2,1)S(1)}, bf16[40,1024]{1,0:T(8,128)(2,1)S(1)}, u32[]{:S(2)}, u32[]{:S(2)}) collective-permute-start(bf16[40,1024]{1,0:T(8,128)(2,1)S(1)} %get-tuple-element.54), channel_id=1, source_target_pairs={{0,80},{8,88},{16,96},{24,104},{32,112},{40,120},{48,0},{56,8},{64... | collective-permute-start | bytes 245768 | tf_op jit(solution)/shard_map/ppermute | solution.py:149
  147.0 8.2 %collective-permute-start.26 = (bf16[40,1024]{1,0:T(8,128)(2,1)S(1)}, bf16[40,1024]{1,0:T(8,128)(2,1)S(1)}, u32[]{:S(2)}, u32[]{:S(2)}) collective-permute-start(bf16[40,1024]{1,0:T(8,128)(2,1)S(1)} %get-tuple-element.55), channel_id=1, source_target_pairs={{0,64},{8,72},{16,80},{24,88},{32,96},{40,104},{48,112},{56,120},{... | collective-permute-start | bytes 245768 | tf_op jit(solution)/shard_map/ppermute | solution.py:149
  152.5 6.9 %collective-permute-start.27 = (bf16[40,1024]{1,0:T(8,128)(2,1)S(1)}, bf16[40,1024]{1,0:T(8,128)(2,1)S(1)}, u32[]{:S(2)}, u32[]{:S(2)}) collective-permute-start(bf16[40,1024]{1,0:T(8,128)(2,1)S(1)} %get-tuple-element.56), channel_id=1, source_target_pairs={{0,48},{8,56},{16,64},{24,72},{32,80},{40,88},{48,96},{56,104},{64... | collective-permute-start | bytes 245768 | tf_op jit(solution)/shard_map/ppermute | solution.py:149
  152.5 6.9 %collective-permute-start.28 = (bf16[40,1024]{1,0:T(8,128)(2,1)S(1)}, bf16[40,1024]{1,0:T(8,128)(2,1)S(1)}, u32[]{:S(2)}, u32[]{:S(2)}) collective-permute-start(bf16[40,1024]{1,0:T(8,128)(2,1)S(1)} %get-tuple-element.57), channel_id=1, source_target_pairs={{0,32},{8,40},{16,48},{24,56},{32,64},{40,72},{48,80},{56,88},{64,... | collective-permute-start | bytes 245768 | tf_op jit(solution)/shard_map/ppermute | solution.py:149
  153.8 6.7 %collective-permute-start.29 = (bf16[40,1024]{1,0:T(8,128)(2,1)S(1)}, bf16[40,1024]{1,0:T(8,128)(2,1)S(1)}, u32[]{:S(2)}, u32[]{:S(2)}) collective-permute-start(bf16[40,1024]{1,0:T(8,128)(2,1)S(1)} %get-tuple-element.58), channel_id=1, source_target_pairs={{0,16},{8,24},{16,32},{24,40},{32,48},{40,56},{48,64},{56,72},{64,... | collective-permute-start | bytes 245768 | tf_op jit(solution)/shard_map/ppermute | solution.py:149
  161.2 14.9 %collective-permute-start.30 = (bf16[128,1024]{1,0:T(8,128)(2,1)S(1)}, bf16[128,1024]{1,0:T(8,128)(2,1)S(1)}, u32[]{:S(2)}, u32[]{:S(2)}) collective-permute-start(bf16[128,1024]{1,0:T(8,128)(2,1)S(1)} %get-tuple-element.60), channel_id=1, source_target_pairs={{0,8},{8,0},{16,24},{24,16},{32,40},{40,32},{48,56},{56,48},{64,72... | collective-permute-start | bytes 786440 | tf_op jit(solution)/shard_map/ppermute | solution.py:145
